TPU v7x, 512 devices: a 4x2x32 block of a 4x8x32 slice. The times are simulated.
512 devices in a mesh: grp: 2 (over y), fs: 32 (over z), tp: 8 (over x, core).
Axes of the slice: x: 4, y: 2, z: 32, core: 2. Of those that a mesh axis runs over, the one named last changes fastest.
The devices are a block of a 4x8x32 slice.
Arguments:
- stream: bfloat16 [64, 128, 2048], P(('grp', 'fs')), parts along dimension 0, may hold values from -6 to 6
- in_gain: float32 [2048], replicated, may hold values from 0.2 to 5
- value_weight: bfloat16 [2048, 1024], P('fs', 'tp'), may hold values from -0.125 to 0.125
- gate_weight: bfloat16 [2048, 1024], P('fs', 'tp'), may hold values from -0.125 to 0.125
- conv_kernel: bfloat16 [31, 1024], P(None, 'tp'), may hold values from -3.6 to 3.6
- conv_gain: float32 [1024], P('tp'), may hold values from 0.1 to 1.9
- conv_shift: float32 [1024], P('tp'), may hold values from -3 to 3
- out_weight: bfloat16 [1024, 2048], P('tp', 'fs'), may hold values from -0.1875 to 0.1875
- norm_gain: float32 [2048], replicated, may hold values from 0.2 to 5
- up_weight: bfloat16 [2048, 8192], P('fs', 'tp'), may hold values from -0.125 to 0.125
- down_weight: bfloat16 [8192, 2048], P('tp', 'fs'), may hold values from -0.0625 to 0.0625
- out_gain: float32 [2048], P('tp'), may hold values from 0.1 to 1.9
Outputs:
- result: bfloat16 [64, 128, 2048], P(('grp', 'fs'), None, 'tp'), parts along dimension 0
There are 2 independent parts, one for each index of `grp`. A program takes and returns all parts, laid end to end along the dimension named above; an argument that names none is the same for every part. Nothing has to cross between parts.
All inputs are finite; a program needn't handle non-finite values.
Results may differ from a plain program's by a relative error of at most 0.02.
Values may be sent and summed in bfloat16 or wider, within the bound.
No kernel may reach another device: no remote copies, remote signals or barrier semaphores. Data moves between devices by JAX's collectives and lax.ppermute only.
A program may use at most 64 MiB of HBM per device.

v0:
```python
import jax
import jax.numpy as jnp
from jax import lax
from jax.sharding import PartitionSpec as P

KW = 31
norm_epsilon = 1e-05
residual_scale = 2.0**0.25


def gather_fs(x):
    groups = lax.axis_size("grp")
    rows = x.shape[0] // groups
    own = lax.dynamic_slice_in_dim(x, lax.axis_index("grp") * rows, rows, 0)
    return lax.all_gather(own, ("fs", "grp"), axis=0, tiled=True)


def norm_rows(values, gain_vector):
    row_mean = jnp.mean(values, axis=-1, keepdims=True)
    row_var = jnp.mean(jnp.square(values - row_mean), axis=-1, keepdims=True)
    return (values - row_mean) * lax.rsqrt(row_var + norm_epsilon) * gain_vector


def contract(left, turned):
    return lax.dot_general(
        left, turned, (((1,), (1,)), ((), ())), preferred_element_type=jnp.float32
    )


def swap_blocks(x):
    return lax.all_to_all(x, "tp", 0, 0, tiled=True)


def summed_tokens(terms):
    tp_count = lax.axis_size("tp")
    tokens, width = terms.shape
    tiles = swap_blocks(terms.astype(jnp.bfloat16).reshape(tp_count, tokens // tp_count, width))
    return jnp.sum(tiles.astype(jnp.float32), axis=0).astype(jnp.bfloat16)


def shards(
    stream,
    in_gain,
    value_weight,
    gate_weight,
    conv_kernel,
    conv_gain,
    conv_shift,
    out_weight,
    norm_gain,
    up_weight,
    down_weight,
    out_gain,
):
    seq_count, seq_length, model_width = stream.shape
    token_count = seq_count * seq_length
    tp_count = lax.axis_size("tp")
    slice_width = model_width // tp_count
    own_tokens = token_count // tp_count
    tp_index = lax.axis_index("tp")
    channels = value_weight.shape[1]
    first = gather_fs(jnp.concatenate([value_weight, gate_weight, out_weight.T], axis=1))
    up_weight, first = lax.optimization_barrier((up_weight, first))
    up_whole = gather_fs(up_weight)
    down_weight, up_whole = lax.optimization_barrier((down_weight, up_whole))
    down_turned = gather_fs(down_weight.T)
    value_gate, out_turned = (first[:, : 2 * channels], first[:, 2 * channels :])
    normed = norm_rows(
        stream.reshape(token_count, model_width).astype(jnp.float32), in_gain
    ).astype(jnp.bfloat16)
    both = jnp.dot(normed, value_gate, preferred_element_type=jnp.float32)
    gated = (both[:, :channels] * jax.nn.sigmoid(both[:, channels:])).astype(jnp.bfloat16)
    convolved = lax.conv_general_dilated(
        gated.reshape(seq_count, seq_length, channels),
        conv_kernel[:, None, :],
        window_strides=(1,),
        padding=[(KW - 1, 0)],
        dimension_numbers=("NWC", "WIO", "NWC"),
        feature_group_count=channels,
        preferred_element_type=jnp.float32,
    ).reshape(token_count, channels)
    sums = jnp.stack([jnp.sum(convolved, axis=1), jnp.sum(convolved * convolved, axis=1)])
    sums = jnp.sum(swap_blocks(jnp.broadcast_to(sums[None], (tp_count, *sums.shape))), axis=0)
    row_mean = sums[0] / (channels * tp_count)
    row_var = sums[1] / (channels * tp_count) - row_mean * row_mean
    activated = jax.nn.silu(
        (convolved - row_mean[:, None]) * lax.rsqrt(row_var + norm_epsilon)[:, None] * conv_gain
        + conv_shift
    ).astype(jnp.bfloat16)
    mixed = summed_tokens(contract(activated, out_turned))
    normed_own = lax.dynamic_slice_in_dim(normed, tp_index * own_tokens, own_tokens, 0)
    settled_own = norm_rows(
        residual_scale * normed_own.astype(jnp.float32) + mixed.astype(jnp.float32), norm_gain
    ).astype(jnp.bfloat16)
    settled = lax.all_gather(settled_own, "tp", axis=0, tiled=True)
    whole_gain = lax.all_gather(out_gain, "tp", axis=0, tiled=True)
    hidden = jnp.square(
        jax.nn.relu(jnp.dot(settled, up_whole, preferred_element_type=jnp.float32))
    ).astype(jnp.bfloat16)
    fed = summed_tokens(contract(hidden, down_turned))
    result_own = norm_rows(
        residual_scale * settled_own.astype(jnp.float32) + fed.astype(jnp.float32), whole_gain
    ).astype(jnp.bfloat16)
    pieces = jnp.moveaxis(result_own.reshape(own_tokens, tp_count, slice_width), 1, 0)
    result = swap_blocks(pieces)
    return result.reshape(seq_count, seq_length, slice_width)


def solution(mesh):
    in_specs = (
        P(("grp", "fs"), None, None),
        P(),
        P("fs", "tp"),
        P("fs", "tp"),
        P(None, "tp"),
        P("tp"),
        P("tp"),
        P("tp", "fs"),
        P(),
        P("fs", "tp"),
        P("tp", "fs"),
        P("tp"),
    )
    out_specs = P(("grp", "fs"), None, "tp")
    return jax.shard_map(shards, mesh=mesh, in_specs=in_specs, out_specs=out_specs, check_vma=False)
```

profile of v0, /device:TPU:33, one launch (start us, length us, event | category | flops | bytes accessed | tf_op | source)
XLA Modules:
  0.0 904.0 jit_solution(4344918902688362367)
XLA Ops:
  6.6 1.4 fusion.28
  8.1 277.9 %all-gather.5.cloned.1.call-done = bf16[2048,384]{1,0:T(8,128)(2,1)} async-done(((bf16[32,384]{1,0:T(8,128)(2,1)}), bf16[2048,384]{1,0:T(8,128)(2,1)}) %all-gather.5.cloned.1.call-update) | async-done | bytes 1572880 | tf_op jit(solution)/shard_map/all_gather | solution.py:15
  286.0 0.6 constant_dynamic-slice_fusion
  286.8 278.4 %all-gather.7.cloned.1.call-done = bf16[2048,1024]{1,0:T(8,128)(2,1)} async-done(((bf16[32,1024]{1,0:T(8,128)(2,1)}), bf16[2048,1024]{1,0:T(8,128)(2,1)}) %all-gather.7.cloned.1.call-update) | async-done | bytes 4194320 | tf_op jit(solution)/shard_map/all_gather | solution.py:15
  565.2 1.5 dynamic-slice_bitcast_fusion
  566.7 1.2 convert_reduce_fusion
  567.9 1.3 fusion.5
  569.3 1.4 fusion.7
  570.7 1.5 fusion.8
  572.3 1.1 fusion.34
  573.5 28.9 %all_to_all.20 = f32[8,2,128]{2,1,0:T(2,128)S(1)} all-to-all(f32[8,2,128]{2,1,0:T(2,128)S(1)} %broadcast_in_dim.5), channel_id=1, replica_groups=mesh['grp'=2,'fs'=32,'tp'=8] {'tp'}, dimensions={0} | all-to-all | bytes 16384 | tf_op jit(solution)/shard_map/all_to_all | solution.py:31
  602.5 2.2 convolution_convert_fusion.1
  604.7 4.1 all-to-all-start.1
  608.8 9.4 %all-to-all-done.1 = bf16[8,16,2048]{2,1,0:T(8,128)(2,1)S(1)} async-done(((bf16[8,16,2048]{2,1,0:T(8,128)(2,1)}), bf16[8,16,2048]{2,1,0:T(8,128)(2,1)S(1)}, u32[]{:S(2)}, u32[]{:S(2)}) %all-to-all-start.1) | async-done | bytes 524320 | tf_op jit(solution)/shard_map/all_to_all | solution.py:31
  618.3 0.1 fusion.12
  618.5 0.2 multiply_reduce_fusion.1
  618.8 14.0 %all_gather.16 = bf16[128,2048]{1,0:T(8,128)(2,1)S(1)} all-gather(bf16[16,2048]{1,0:T(8,128)(2,1)S(1)} %multiply_convert_fusion.1), channel_id=1, replica_groups=mesh['grp'=2,'fs'=32,'tp'=8] {'tp'}, dimensions={0}, use_global_device_ids=true | all-gather | bytes 589824 | tf_op jit(solution)/shard_map/all_gather | solution.py:95
  632.8 211.7 %all-gather.9.cloned.1.call-done = bf16[2048,1024]{1,0:T(8,128)(2,1)} async-done(((bf16[32,1024]{1,0:T(8,128)(2,1)}), bf16[2048,1024]{1,0:T(8,128)(2,1)}) %all-gather.9.cloned.1.call-update) | async-done | bytes 4194320 | tf_op jit(solution)/shard_map/all_gather | solution.py:15
  844.5 6.4 convolution_convert_fusion
  850.8 24.9 %all-to-all-start.2 = ((bf16[8,16,2048]{2,1,0:T(8,128)(2,1)}), bf16[8,16,2048]{2,1,0:T(8,128)(2,1)S(1)}, u32[]{:S(2)}, u32[]{:S(2)}) async-start(bf16[8,16,2048]{2,1,0:T(8,128)(2,1)} %bitcast.11), calls=%async_computation.2 | async-start | bytes 1048576 | tf_op jit(solution)/shard_map/all_to_all | solution.py:31
  875.7 13.1 %all-gather = f32[8,1,256]{2,1,0:T(1,128)S(1)} all-gather(f32[1,1,256]{2,1,0:T(1,128)S(1)} %bitcast.57), channel_id=1, replica_groups=mesh['grp'=2,'fs'=32,'tp'=8] {'tp'}, dimensions={0}, use_global_device_ids=true | all-gather | bytes 9216 | tf_op jit(solution)/shard_map/all_gather | solution.py:96
  889.1 0.2 multiply_reduce_fusion
  889.4 7.4 all_to_all.21
  896.8 0.6 copy.41
  (38 shorter events, 1.1 us)
Async XLA Ops:
  6.5 279.5 %copy-start = (bf16[64,1024]{1,0:T(8,128)(2,1)S(1)}, bf16[64,1024]{1,0:T(8,128)(2,1)}, u32[]{:S(2)}) copy-start(bf16[64,1024]{1,0:T(8,128)(2,1)} %param.21) | copy-start | bytes 393220
  6.6 565.7 %copy-start.5 = (bf16[31,128]{1,0:T(8,128)(2,1)S(1)}, bf16[31,128]{1,0:T(8,128)(2,1)}, u32[]{:S(2)}) copy-start(bf16[31,128]{1,0:T(8,128)(2,1)} %param.16) | copy-start | bytes 23812
  6.6 595.9 %copy-start.4 = (f32[128]{0:T(128)S(1)}, f32[128]{0:T(128)}, u32[]{:S(2)}) copy-start(f32[128]{0:T(128)} %param.17) | copy-start | bytes 1540
  6.6 595.9 %copy-start.3 = (f32[128]{0:T(128)S(1)}, f32[128]{0:T(128)}, u32[]{:S(2)}) copy-start(f32[128]{0:T(128)} %param.18) | copy-start | bytes 1540
  6.6 279.5 %all-gather.5.cloned.1.call-start = ((), (), s32[]{:S(2)}) async-start(), calls=%async_computation.4 | async-start | bytes 1597440 | tf_op jit(solution)/shard_map/all_gather | solution.py:15
  8.1 557.1 %all-gather.7.cloned.1.call-start = ((), (), s32[]{:S(2)}) async-start(), calls=%async_computation.5 | async-start | bytes 4259840 | tf_op jit(solution)/shard_map/all_gather | solution.py:15
  286.7 557.7 %all-gather.9.cloned.1.call-start = ((), (), s32[]{:S(2)}) async-start(), calls=%async_computation.6 | async-start | bytes 4259840 | tf_op jit(solution)/shard_map/all_gather | solution.py:15
  566.7 52.0 %copy-start.1 = (f32[2048]{0:T(1024)S(1)}, f32[2048]{0:T(1024)}, u32[]{:S(2)}) copy-start(f32[2048]{0:T(1024)} %param.20) | copy-start | bytes 24580
  604.7 13.5 %all-to-all-start.1 = ((bf16[8,16,2048]{2,1,0:T(8,128)(2,1)}), bf16[8,16,2048]{2,1,0:T(8,128)(2,1)S(1)}, u32[]{:S(2)}, u32[]{:S(2)}) async-start(bf16[8,16,2048]{2,1,0:T(8,128)(2,1)} %bitcast.9), calls=%async_computation.1 | async-start | bytes 1048576 | tf_op jit(solution)/shard_map/all_to_all | solution.py:31
  632.8 243.0 %copy-start.2 = (f32[256]{0:T(256)S(1)}, f32[256]{0:T(256)}, u32[]{:S(2)}) copy-start(f32[256]{0:T(256)} %param.23) | copy-start | bytes 3076
  850.8 38.0 %all-to-all-start.2 = ((bf16[8,16,2048]{2,1,0:T(8,128)(2,1)}), bf16[8,16,2048]{2,1,0:T(8,128)(2,1)S(1)}, u32[]{:S(2)}, u32[]{:S(2)}) async-start(bf16[8,16,2048]{2,1,0:T(8,128)(2,1)} %bitcast.11), calls=%async_computation.2 | async-start | bytes 1048576 | tf_op jit(solution)/shard_map/all_to_all | solution.py:31
Sparse Core Ops, SparseCore 0:
  10.5 275.4 all-gather.4
  289.2 275.9 all-gather.6
  568.3 276.0 all-gather.8
where the time goes:
time: 905 us; the launch traced here: 904 us
  waiting for transfers between devices  778 us (86%)
  blocking collectives  63.5 us (7%)
  starting transfers between devices  29.2 us (3%)
  between operations  13.3 us (1%)
  matrix products  11.2 us (1%)
    all_gather x3, waiting for transfers between devices, gather_fs(): return lax.all_gather(own, ('fs', 'grp'), axis=0, tiled=True)  768 us
    all_to_all x2, blocking collectives, swap_blocks(): return lax.all_to_all(x, 'tp', 0, 0, tiled=True)  36.4 us
    all_to_all x2, starting transfers between devices, swap_blocks(): return lax.all_to_all(x, 'tp', 0, 0, tiled=True)  29 us
  transfers between devices with their start and end apart: 5, of which 4 were waited for; matrix products, arithmetic and copies ran while one was open for 1% of the time, Pallas kernels for 0%

commit v1 on v0

--- a/solution.py
+++ b/solution.py
@@ -8,11 +8,16 @@
 residual_scale = 2.0**0.25
 
 
+def all_by_exchange(block, name, d):
+    repeated = jnp.stack([block] * lax.axis_size(name))
+    return jnp.concatenate(lax.all_to_all(repeated, name, 0, 0), axis=d)
+
+
 def gather_fs(x):
     groups = lax.axis_size("grp")
     rows = x.shape[0] // groups
     own = lax.dynamic_slice_in_dim(x, lax.axis_index("grp") * rows, rows, 0)
-    return lax.all_gather(own, ("fs", "grp"), axis=0, tiled=True)
+    return all_by_exchange(own, ("fs", "grp"), 0)
 
 
 def norm_rows(values, gain_vector):

time: 905 us -> 1040 us (1.15)
  waiting for transfers between devices: 778 us -> 886 us
  starting transfers between devices: 29.2 us -> 99.2 us
  blocking collectives: 63.5 us -> 34.6 us
  between operations: 13.3 us -> 0.19 us
    all_to_all x0 -> x3, waiting for transfers between devices: none -> 872 us  [all_by_exchange(): return jnp.concatenate(lax.all_to_all(repeated, name, 0, 0), axis=d)]
    all_gather x3 -> x0, waiting for transfers between devices: 768 us -> none  [gather_fs(): return lax.all_gather(own, ('fs', 'grp'), axis=0, tiled=True)]
    all_to_all x0 -> x3, starting transfers between devices: none -> 64.3 us  [all_by_exchange(): return jnp.concatenate(lax.all_to_all(repeated, name, 0, 0), axis=d)]
    all_to_all x2 -> x1, blocking collectives: 36.4 us -> 7.45 us  [swap_blocks(): return lax.all_to_all(x, 'tp', 0, 0, tiled=True)]
    all_to_all x2 -> x3, starting transfers between devices: 29 us -> 34.9 us  [swap_blocks(): return lax.all_to_all(x, 'tp', 0, 0, tiled=True)]
  transfers between devices with their start and end apart: 5 -> 6, of which waited for: 4 -> 5; matrix products, arithmetic and copies ran while one was open for 1% -> 0% of each run, Pallas kernels for 0% -> 0%
where the time goes in v1:
time: 1040 us
  waiting for transfers between devices  886 us (85%)
  starting transfers between devices  99.2 us (10%)
  blocking collectives  34.6 us (3%)
    all_to_all x3, waiting for transfers between devices, all_by_exchange(): return jnp.concatenate(lax.all_to_all(repeated, name, 0, 0), axis=d)  872 us
    all_to_all x3, starting transfers between devices, all_by_exchange(): return jnp.concatenate(lax.all_to_all(repeated, name, 0, 0), axis=d)  64.3 us
    all_to_all x3, starting transfers between devices, swap_blocks(): return lax.all_to_all(x, 'tp', 0, 0, tiled=True)  34.9 us
  transfers between devices with their start and end apart: 6, of which 5 were waited for; matrix products, arithmetic and copies ran while one was open for 0% of the time, Pallas kernels for 0%

profile of v1, /device:TPU:33, one launch (start us, length us, event | category | flops | bytes accessed | tf_op | source)
XLA Modules:
  0.0 1039.5 jit_solution(9497518872053203041)
XLA Ops:
  0.0 0.8 fusion.28
  0.8 1.3 stack.12
  2.1 49.4 %all-to-all-start = ((bf16[64,32,384]{2,1,0:T(8,128)(2,1)}), bf16[64,32,384]{2,1,0:T(8,128)(2,1)S(1)}, u32[]{:S(2)}, u32[]{:S(2)}) async-start(bf16[64,32,384]{2,1,0:T(8,128)(2,1)} %stack.12), calls=%async_computation | async-start | bytes 3145728 | tf_op jit(solution)/shard_map/all_to_all | solution.py:13
  52.0 0.4 fusion.7
  52.4 148.0 %all-to-all-done = bf16[64,32,384]{2,1,0:T(8,128)(2,1)S(1)} async-done(((bf16[64,32,384]{2,1,0:T(8,128)(2,1)}), bf16[64,32,384]{2,1,0:T(8,128)(2,1)S(1)}, u32[]{:S(2)}, u32[]{:S(2)}) %all-to-all-start) | async-done | bytes 1572896 | tf_op jit(solution)/shard_map/all_to_all | solution.py:13
  200.8 1.1 fusion.34
  202.0 0.6 broadcast_in_dim.5
  202.6 9.9 all-to-all-start.1
  212.5 4.6 all-to-all-done.1
  217.1 2.5 stack.16
  219.7 7.4 all-to-all-start.3
  227.1 1.2 convolution_convert_fusion.1
  228.4 368.4 %all-to-all-done.3 = bf16[64,32,1024]{2,1,0:T(8,128)(2,1)} async-done(((bf16[64,32,1024]{2,1,0:T(8,128)(2,1)}), bf16[64,32,1024]{2,1,0:T(8,128)(2,1)}, u32[]{:S(2)}, u32[]{:S(2)}) %all-to-all-start.3) | async-done | bytes 4194336 | tf_op jit(solution)/shard_map/all_to_all | solution.py:13
  596.7 12.8 %all-to-all-start.2 = ((bf16[8,16,2048]{2,1,0:T(8,128)(2,1)}), bf16[8,16,2048]{2,1,0:T(8,128)(2,1)S(1)}, u32[]{:S(2)}, u32[]{:S(2)}) async-start(bf16[8,16,2048]{2,1,0:T(8,128)(2,1)} %bitcast.10), calls=%async_computation.2 | async-start | bytes 1048576 | tf_op jit(solution)/shard_map/all_to_all | solution.py:36
  609.5 9.4 all-to-all-done.2
  618.9 2.5 stack.17
  621.4 7.4 all-to-all-start.4
  629.4 14.0 %all_gather.6 = bf16[128,2048]{1,0:T(8,128)(2,1)S(1)} all-gather(bf16[16,2048]{1,0:T(8,128)(2,1)S(1)} %multiply_convert_fusion.1), channel_id=1, replica_groups=mesh['grp'=2,'fs'=32,'tp'=8] {'tp'}, dimensions={0}, use_global_device_ids=true | all-gather | bytes 589824 | tf_op jit(solution)/shard_map/all_gather | solution.py:100
  643.4 355.7 %all-to-all-done.4 = bf16[64,32,1024]{2,1,0:T(8,128)(2,1)} async-done(((bf16[64,32,1024]{2,1,0:T(8,128)(2,1)}), bf16[64,32,1024]{2,1,0:T(8,128)(2,1)}, u32[]{:S(2)}, u32[]{:S(2)}) %all-to-all-start.4) | async-done | bytes 4194336 | tf_op jit(solution)/shard_map/all_to_all | solution.py:13
  999.1 6.4 convolution_convert_fusion
  1005.5 12.2 %all-to-all-start.5 = ((bf16[8,16,2048]{2,1,0:T(8,128)(2,1)}), bf16[8,16,2048]{2,1,0:T(8,128)(2,1)S(1)}, u32[]{:S(2)}, u32[]{:S(2)}) async-start(bf16[8,16,2048]{2,1,0:T(8,128)(2,1)} %bitcast.14), calls=%async_computation.5 | async-start | bytes 1048576 | tf_op jit(solution)/shard_map/all_to_all | solution.py:36
  1017.7 13.2 %all-gather = f32[8,1,256]{2,1,0:T(1,128)S(1)} all-gather(f32[1,1,256]{2,1,0:T(1,128)S(1)} %bitcast.62), channel_id=1, replica_groups=mesh['grp'=2,'fs'=32,'tp'=8] {'tp'}, dimensions={0}, use_global_device_ids=true | all-gather | bytes 9216 | tf_op jit(solution)/shard_map/all_gather | solution.py:101
  1031.5 7.4 all_to_all.35
  1038.9 0.6 copy.41
  (45 shorter events, 2.0 us)
Async XLA Ops:
  0.0 212.5 %copy-start = (bf16[64,1024]{1,0:T(8,128)(2,1)S(1)}, bf16[64,1024]{1,0:T(8,128)(2,1)}, u32[]{:S(2)}) copy-start(bf16[64,1024]{1,0:T(8,128)(2,1)} %param.21) | copy-start | bytes 393220
  0.0 51.5 %copy-start.1 = (bf16[1,128,2048]{2,1,0:T(8,128)(2,1)S(1)}, bf16[1,128,2048]{2,1,0:T(8,128)(2,1)}, u32[]{:S(2)}) copy-start(bf16[1,128,2048]{2,1,0:T(8,128)(2,1)} %param.12) | copy-start | bytes 1572868
  0.0 52.0 %copy-start.3 = (f32[2048]{0:T(1024)S(1)}, f32[2048]{0:T(1024)}, u32[]{:S(2)}) copy-start(f32[2048]{0:T(1024)} %param.13) | copy-start | bytes 24580
  0.8 200.0 %copy-start.8 = (bf16[31,128]{1,0:T(8,128)(2,1)S(1)}, bf16[31,128]{1,0:T(8,128)(2,1)}, u32[]{:S(2)}) copy-start(bf16[31,128]{1,0:T(8,128)(2,1)} %param.16) | copy-start | bytes 23812
  2.1 198.3 %all-to-all-start = ((bf16[64,32,384]{2,1,0:T(8,128)(2,1)}), bf16[64,32,384]{2,1,0:T(8,128)(2,1)S(1)}, u32[]{:S(2)}, u32[]{:S(2)}) async-start(bf16[64,32,384]{2,1,0:T(8,128)(2,1)} %stack.12), calls=%async_computation | async-start | bytes 3145728 | tf_op jit(solution)/shard_map/all_to_all | solution.py:13
  202.6 14.5 %all-to-all-start.1 = ((f32[8,2,128]{2,1,0:T(2,128)}), f32[8,2,128]{2,1,0:T(2,128)S(1)}, u32[]{:S(2)}, u32[]{:S(2)}) async-start(f32[8,2,128]{2,1,0:T(2,128)} %broadcast_in_dim.5), calls=%async_computation.1 | async-start | bytes 16384 | tf_op jit(solution)/shard_map/all_to_all | solution.py:36
  219.6 7.5 copy-start.6
  219.7 7.5 copy-start.7
  219.7 389.8 %copy-start.2 = (bf16[1024,64]{0,1:T(8,128)(2,1)S(1)}, bf16[1024,64]{0,1:T(8,128)(2,1)}, u32[]{:S(2)}) copy-start(bf16[1024,64]{0,1:T(8,128)(2,1)} %param.22) | copy-start | bytes 393220
  219.7 377.1 %all-to-all-start.3 = ((bf16[64,32,1024]{2,1,0:T(8,128)(2,1)}), bf16[64,32,1024]{2,1,0:T(8,128)(2,1)}, u32[]{:S(2)}, u32[]{:S(2)}) async-start(bf16[64,32,1024]{2,1,0:T(8,128)(2,1)} %stack.16), calls=%async_computation.3 | async-start | bytes 8388608 | tf_op jit(solution)/shard_map/all_to_all | solution.py:13
  596.7 22.2 %all-to-all-start.2 = ((bf16[8,16,2048]{2,1,0:T(8,128)(2,1)}), bf16[8,16,2048]{2,1,0:T(8,128)(2,1)S(1)}, u32[]{:S(2)}, u32[]{:S(2)}) async-start(bf16[8,16,2048]{2,1,0:T(8,128)(2,1)} %bitcast.10), calls=%async_computation.2 | async-start | bytes 1048576 | tf_op jit(solution)/shard_map/all_to_all | solution.py:36
  621.4 7.9 copy-start.4
  621.4 377.6 %all-to-all-start.4 = ((bf16[64,32,1024]{2,1,0:T(8,128)(2,1)}), bf16[64,32,1024]{2,1,0:T(8,128)(2,1)}, u32[]{:S(2)}, u32[]{:S(2)}) async-start(bf16[64,32,1024]{2,1,0:T(8,128)(2,1)} %stack.17), calls=%async_computation.4 | async-start | bytes 8388608 | tf_op jit(solution)/shard_map/all_to_all | solution.py:13
  999.1 18.6 %copy-start.5 = (f32[256]{0:T(256)S(1)}, f32[256]{0:T(256)}, u32[]{:S(2)}) copy-start(f32[256]{0:T(256)} %param.23) | copy-start | bytes 3076
  1005.5 25.4 %all-to-all-start.5 = ((bf16[8,16,2048]{2,1,0:T(8,128)(2,1)}), bf16[8,16,2048]{2,1,0:T(8,128)(2,1)S(1)}, u32[]{:S(2)}, u32[]{:S(2)}) async-start(bf16[8,16,2048]{2,1,0:T(8,128)(2,1)} %bitcast.14), calls=%async_computation.5 | async-start | bytes 1048576 | tf_op jit(solution)/shard_map/all_to_all | solution.py:36
